TPU v7x, 256 devices: a whole 4x4x8 slice. The times are simulated.
256 devices in a mesh: ep: 16 (over y, x), tp: 16 (over z, core).
Axes of the slice: x: 4, y: 4, z: 8, core: 2. Of those that a mesh axis runs over, the one named last changes fastest.
Arguments:
- queries: bfloat16 [2, 1024, 16384], P(None, 'tp', 'ep'), may hold values from -6 to 6
- key_vectors: bfloat16 [2, 1024, 16384], P(None, 'tp', 'ep'), may hold values from -6 to 6
- value_vectors: bfloat16 [2, 1024, 16384], P(None, 'tp', 'ep'), may hold values from -12 to 12
- cumulative_gate: float32 [2, 16, 16384], P(None, 'tp'), may hold values from -16384 to 0, as said below
- expert_input: bfloat16 [32768, 2048], P(('ep', 'tp')), may hold values from -6 to 6
- norm_gain: float32 [2048], replicated, may hold values from 0.1 to 1.9
- group_choice: int32 [32768], P(('ep', 'tp')), may hold values from 0 to 15, as said below
- group_weight: float32 [32768], P(('ep', 'tp')), may hold values from 0.3 to 1
- expert_logits: float32 [32768, 2], P(('ep', 'tp')), may hold values from -6 to 6
- gate_weight: bfloat16 [32, 2048, 2048], P('ep', 'tp'), may hold values from -0.125 to 0.125
- up_weight: bfloat16 [32, 2048, 2048], P('ep', 'tp'), may hold values from -0.125 to 0.125
- down_weight: bfloat16 [32, 2048, 2048], P('ep', 'tp'), may hold values from -0.25 to 0.25
Outputs:
- attention: bfloat16 [2, 1024, 16384], P(None, 'tp', 'ep')
- expert_output: bfloat16 [32768, 2048], P(('ep', 'tp'))
Inputs may be any that keep to these rules, and one draw needn't show every extreme that they name: `cumulative_gate`: each row is non-increasing along positions. `group_choice`: in each aligned block of 128 rows (the rows of one device) no group is named more than 10 times, and one group is named exactly 10 times in every block.
All inputs are finite; a program needn't handle non-finite values.
Results may differ from a plain program's by a relative error of at most 0.017.
Values may be sent and summed in bfloat16 or wider, within the bound.
A program may use at most 128 MiB of HBM per device.

v0:
```python
from functools import partial
import math

import jax
import jax.numpy as jnp
from jax import lax
from jax.sharding import PartitionSpec as P

neg_fill = -1e30
norm_eps = 1e-06


def partner(x, axis, distance):
    return lax.ppermute(x, axis, [(i, i ^ 1 << distance) for i in range(lax.axis_size(axis))])


def sent_together(arrays, axis, dim, along):
    ends, at = ([], 0)
    for a in arrays[:-1]:
        at += a.shape[along]
        ends.append(at)
    both = jnp.concatenate(arrays, axis=along)
    return tuple(jnp.split(lax.all_gather(both, axis, axis=dim, tiled=True), ends, axis=along))


def side_by_side(arrays, axis, split_dim, concat_dim, along):
    both = jnp.concatenate(arrays, axis=along)
    whole, at, outs = (
        lax.all_to_all(both, axis, split_axis=split_dim, concat_axis=concat_dim, tiled=True),
        0,
        [],
    )
    for a in arrays:
        outs.append(lax.slice_in_dim(whole, at, at + a.shape[along], axis=along))
        at += a.shape[along]
    return tuple(outs)


def unchanged(running):
    return running


def attend(queries, key_vectors, value_vectors, cumulative_gate):
    seq_count, feat_width, seg_len = queries.shape
    heads_here = cumulative_gate.shape[1]
    head_dim = feat_width // heads_here
    half_len = seg_len // 2
    ep_size = lax.axis_size("ep")
    ep_rank = lax.axis_index("ep")
    score_scale = 1.0 / math.sqrt(head_dim)
    query_grid = queries.reshape(seq_count, heads_here, head_dim, seg_len)
    early_half = query_grid[:, :, :, :half_len]
    later_half = query_grid[:, :, :, half_len:]
    early_start = ep_rank * seg_len
    for bit_index in range(ep_size.bit_length() - 1):
        later_half = partner(later_half, "ep", bit_index)
    later_start = (ep_size - 1 - ep_rank) * seg_len + half_len
    halves = ((early_half, early_start), (later_half, later_start))
    query_gates = [
        lax.dynamic_slice_in_dim(cumulative_gate, early_start, half_len, 2),
        lax.dynamic_slice_in_dim(cumulative_gate, later_start, half_len, 2),
    ]

    def absorb(running, key_block, value_block, gate_block, key_start, half_index):
        query_block, query_start = halves[half_index]
        peak_old, total_old, acc_old = running
        scores = (
            jnp.einsum(
                "shdq,shdk->shqk", query_block, key_block, preferred_element_type=jnp.float32
            )
            * score_scale
        )
        scores = scores + query_gates[half_index][:, :, :, None] - gate_block[:, :, None, :]
        query_pos = query_start + jnp.arange(half_len, dtype=jnp.int32)
        key_pos = key_start + jnp.arange(key_block.shape[3], dtype=jnp.int32)
        allowed = key_pos[None, :] <= query_pos[:, None]
        scores = jnp.where(allowed, scores, neg_fill)
        peak_new = jnp.maximum(peak_old, jnp.max(scores, axis=3))
        shrink = jnp.exp(peak_old - peak_new)
        weights = jnp.where(allowed, jnp.exp(scores - peak_new[:, :, :, None]), 0.0)
        total_new = total_old * shrink + jnp.sum(weights, axis=3)
        acc_new = acc_old * shrink[:, :, None, :] + jnp.einsum(
            "shqk,shdk->shdq",
            weights.astype(jnp.bfloat16),
            value_block,
            preferred_element_type=jnp.float32,
        )
        return (peak_new, total_new, acc_new)

    blank_state = (
        jnp.full((seq_count, heads_here, half_len), neg_fill, jnp.float32),
        jnp.zeros((seq_count, heads_here, half_len), jnp.float32),
        jnp.zeros((seq_count, heads_here, head_dim, half_len), jnp.float32),
    )
    key_piece, value_piece = sent_together((key_vectors, value_vectors), "ep", 2, 0)
    length = key_piece.shape[2]
    key_span = math.gcd(length, 1024)

    def visit_block(counter, inner):
        offset = counter * key_span
        key_block = lax.dynamic_slice_in_dim(key_piece, offset, key_span, 2).reshape(
            seq_count, heads_here, head_dim, key_span
        )
        value_block = lax.dynamic_slice_in_dim(value_piece, offset, key_span, 2).reshape(
            seq_count, heads_here, head_dim, key_span
        )
        gate_block = lax.dynamic_slice_in_dim(cumulative_gate, offset, key_span, 2)
        updated = []
        for half_index in range(2):
            last_pos = halves[half_index][1] + half_len - 1
            step_fn = partial(
                absorb,
                key_block=key_block,
                value_block=value_block,
                gate_block=gate_block,
                key_start=offset,
                half_index=half_index,
            )
            updated.append(lax.cond(offset <= last_pos, step_fn, unchanged, inner[half_index]))
        return tuple(updated)

    states = lax.fori_loop(0, length // key_span, visit_block, (blank_state, blank_state))
    outputs = []
    for half_index in range(2):
        acc_final = states[half_index][2]
        total_final = states[half_index][1]
        outputs.append((acc_final / total_final[:, :, None, :]).astype(jnp.bfloat16))
    later_out = outputs[1]
    for bit_index in range(ep_size.bit_length() - 1):
        later_out = partner(later_out, "ep", bit_index)
    return jnp.concatenate([outputs[0], later_out], axis=3).reshape(seq_count, feat_width, seg_len)


def expert_hidden(row_block, route_block, gate_weight, up_weight):
    gate_act = jnp.einsum("rd,efd->ref", row_block, gate_weight, preferred_element_type=jnp.float32)
    up_act = jnp.einsum("rd,efd->ref", row_block, up_weight, preferred_element_type=jnp.float32)
    return (jax.nn.silu(gate_act) * up_act * route_block.astype(jnp.float32)[:, :, None]).astype(
        jnp.bfloat16
    )


def mixture(
    expert_input,
    norm_gain,
    group_choice,
    group_weight,
    expert_logits,
    gate_weight,
    up_weight,
    down_weight,
):
    tok_rows, model_dim = expert_input.shape
    group_size = gate_weight.shape[0]
    ep_size = lax.axis_size("ep")
    capacity = 5 * tok_rows // (4 * ep_size)
    token_float = expert_input.astype(jnp.float32)
    normed = (
        token_float
        * lax.rsqrt(jnp.mean(token_float * token_float, axis=1, keepdims=True) + norm_eps)
        * norm_gain
    ).astype(jnp.bfloat16)
    routing = (group_weight[:, None] * jax.nn.softmax(expert_logits, axis=1)).astype(jnp.bfloat16)
    member = (group_choice[:, None] == jnp.arange(ep_size, dtype=jnp.int32)[None, :]).astype(
        jnp.int32
    )
    before = jnp.cumsum(member, axis=0) - member
    slot_index = jnp.sum(before * member, axis=1)
    flat_slot = group_choice * capacity + slot_index
    places = (
        flat_slot[None, :] == jnp.arange(ep_size * capacity, dtype=jnp.int32)[:, None]
    ).astype(jnp.bfloat16)
    outgoing = (
        jnp.dot(places, normed, preferred_element_type=jnp.float32)
        .astype(jnp.bfloat16)
        .reshape(ep_size, capacity, model_dim)
    )
    send_route = (
        jnp.dot(places, routing, preferred_element_type=jnp.float32)
        .astype(jnp.bfloat16)
        .reshape(ep_size, capacity, group_size)
    )
    arrived, arrived_route = side_by_side((outgoing, send_route), "ep", 0, 0, 2)
    local_rows = arrived.reshape(ep_size * capacity, model_dim)
    local_route = arrived_route.reshape(ep_size * capacity, group_size)
    gathered_rows, gathered_route = sent_together((local_rows, local_route), "tp", 0, 1)
    hidden = expert_hidden(gathered_rows, gathered_route, gate_weight, up_weight)
    summed = lax.psum_scatter(
        jnp.einsum("ref,efd->rd", hidden, down_weight, preferred_element_type=jnp.float32).astype(
            jnp.bfloat16
        ),
        "tp",
        scatter_dimension=0,
        tiled=True,
    )
    returned = lax.all_to_all(
        summed.reshape(ep_size, capacity, model_dim), "ep", split_axis=0, concat_axis=0, tiled=True
    )
    returned_flat = returned.reshape(ep_size * capacity, model_dim)
    return jnp.einsum(
        "pt,pd->td", places, returned_flat, preferred_element_type=jnp.float32
    ).astype(jnp.bfloat16)


def local(
    queries,
    key_vectors,
    value_vectors,
    cumulative_gate,
    expert_input,
    norm_gain,
    group_choice,
    group_weight,
    expert_logits,
    gate_weight,
    up_weight,
    down_weight,
):
    attention = attend(queries, key_vectors, value_vectors, cumulative_gate)
    expert_output = mixture(
        expert_input,
        norm_gain,
        group_choice,
        group_weight,
        expert_logits,
        gate_weight,
        up_weight,
        down_weight,
    )
    return (attention, expert_output)


def solution(mesh):
    return jax.shard_map(
        local,
        mesh=mesh,
        in_specs=(
            P(None, "tp", "ep"),
            P(None, "tp", "ep"),
            P(None, "tp", "ep"),
            P(None, "tp", None),
            P(("ep", "tp"), None),
            P(),
            P(("ep", "tp")),
            P(("ep", "tp")),
            P(("ep", "tp"), None),
            P("ep", "tp", None),
            P("ep", "tp", None),
            P("ep", "tp", None),
        ),
        out_specs=(P(None, "tp", "ep"), P(("ep", "tp"), None)),
        check_vma=False,
    )
```

profile of v0, /device:TPU:24, one launch (start us, length us, event | category | flops | bytes accessed | tf_op | source)
XLA Modules:
  0.0 357.9 jit_solution(16972073377702757133)
XLA Ops:
  15.3 23.0 %all_to_all.10 = bf16[16,10,2050]{2,1,0:T(8,128)(2,1)S(1)} all-to-all(bf16[16,10,2050]{2,1,0:T(8,128)(2,1)S(1)} %pad_maximum_fusion), channel_id=1, replica_groups=mesh['ep'=16,'tp'=16] {'ep'}, dimensions={0} | all-to-all | bytes 1312000 | tf_op jit(solution)/shard_map/all_to_all | solution.py:29
  39.5 2.0 pad_maximum_fusion.1
  43.5 67.8 %all-gather.5.cloned.1.call-done = bf16[2560,2050]{1,0:T(8,128)(2,1)} async-done(((bf16[160,2050]{1,0:T(8,128)(2,1)}), bf16[2560,2050]{1,0:T(8,128)(2,1)}) %all-gather.5.cloned.1.call-update) | async-done | bytes 10496016 | tf_op jit(solution)/shard_map/all_gather | solution.py:23
  112.8 7.1 %fusion.41 = f32[2560,2,128]{2,0,1:T(8,128)} fusion(bf16[2,128,2048]{2,1,0:T(8,128)(2,1)S(1)} %copy-done.5, bf16[2560,2050]{1,0:T(8,128)(2,1)} %all-gather.5.cloned.1.call-done), kind=kOutput, calls=%fused_computation.52 | convolution fusion | flops 2684354560 | bytes 14155776 | tf_op jit(solution)/shard_map/rd,efd->ref/dot_general | solution.py:135
  120.0 16.4 %bitcast_convert_fusion = bf16[2560,2048]{1,0:T(8,128)(2,1)} fusion(bf16[2,128,2048]{2,1,0:T(8,128)(2,1)S(1)} %copy-done, bf16[2,128,2048]{2,1,0:T(8,128)(2,1)} %param.28, bf16[2560,2050]{1,0:T(8,128)(2,1)} %all-gather.5.cloned.1.call-done, f32[2560,2,128]{2,0,1:T(8,128)} %fusion.41, f32[2560,2]{0,1:T(2,128)S(1)} %convert_element_type.73), kind=kOutput, calls=%fused_computation.49 | convolution fusion | flops 5378539520 | bytes 25710592 | tf_op jit(solution)/shard_map/ref,efd->rd/dot_general | solution.py:188
  138.9 4.2 %collective-permute-done = bf16[2,1,64,512]{3,2,0,1:T(8,128)(2,1)S(1)} collective-permute-done((bf16[2,1,64,512]{3,2,0,1:T(8,128)(2,1)S(1)}, bf16[2,1,64,512]{3,2,0,1:T(8,128)(2,1)S(1)}, u32[]{:S(2)}, u32[]{:S(2)}) %collective-permute-start) | collective-permute-done | bytes 131104 | tf_op jit(solution)/shard_map/ppermute | solution.py:14
  143.1 3.0 collective-permute-start.1
  146.1 3.5 collective-permute-done.1
  150.6 6.9 %collective-permute-done.2 = bf16[2,1,64,512]{3,2,0,1:T(8,128)(2,1)S(1)} collective-permute-done((bf16[2,1,64,512]{3,2,0,1:T(8,128)(2,1)S(1)}, bf16[2,1,64,512]{3,2,0,1:T(8,128)(2,1)S(1)}, u32[]{:S(2)}, u32[]{:S(2)}) %collective-permute-start.2) | collective-permute-done | bytes 131104 | tf_op jit(solution)/shard_map/ppermute | solution.py:14
  158.7 32.8 %all-gather.3.cloned.1.call-done = bf16[4,64,16384]{2,1,0:T(8,128)(2,1)} async-done(((bf16[4,64,1024]{2,1,0:T(8,128)(2,1)}), bf16[4,64,16384]{2,1,0:T(8,128)(2,1)}) %all-gather.3.cloned.1.call-update) | async-done | bytes 8388624 | tf_op jit(solution)/shard_map/all_gather | solution.py:23
  191.6 5.8 %fusion.59 = (bf16[2,64,16384]{2,1,0:T(8,128)(2,1)}, bf16[2,64,16384]{2,1,0:T(8,128)(2,1)}) fusion(bf16[4,64,16384]{2,1,0:T(8,128)(2,1)} %all-gather.3.cloned.1.call-done), kind=kLoop, calls=%fused_computation.89 | loop fusion | bytes 16777216 | tf_op jit(solution)/shard_map/split | solution.py:23
  197.5 113.8 %while.26 = (s32[]{:T(128)}, f32[2,1,512]{2,0,1:T(2,128)S(1)}, f32[2,1,512]{2,0,1:T(2,128)S(1)}, f32[2,1,64,512]{3,2,0,1:T(8,128)S(1)}, f32[2,1,512]{2,0,1:T(2,1...) while((s32[]{:T(128)}, f32[2,1,512]{2,0,1:T(2,128)S(1)}, ...), condition=%wide.region_9.10_spmd, body=%wide.region_0.9_spmd.sunk | while | flops 578036736 | bytes 33014324 | solution.py:122
  198.6 5.6 %conditional.4 = ((f32[2,1,512]{2,0,1:T(2,128)S(1)}, f32[2,1,512]{2,0,1:T(2,128)S(1)}, f32[2,1,64,512]{3,2,0,1:T(8,128)S(1)})) conditional(s32[]{:T(128)} %convert_element_type.118, (f32[2,1,512]{2,0,1:T(2,128)S(1)}, f32[2,1,512]{2,0,1:T(2,128)S(1)}, f32[2,1,64,512]{3,2,0,1:T(8,128)S(1)}) %tuple.74, (s32[]{:T(128)}, s32[]{:T(128)}, ...), branch_computations={%region_1.0_spmd, %region_2.4_spmd} | conditional | flops 289018368 | bytes 15974440 | solution.py:119
  202.2 2.0 fusion.1
  204.2 5.6 %conditional.5 = ((f32[2,1,512]{2,0,1:T(2,128)S(1)}, f32[2,1,512]{2,0,1:T(2,128)S(1)}, f32[2,1,64,512]{3,2,0,1:T(8,128)S(1)})) conditional(s32[]{:T(128)} %convert_element_type.119, (f32[2,1,512]{2,0,1:T(2,128)S(1)}, f32[2,1,512]{2,0,1:T(2,128)S(1)}, f32[2,1,64,512]{3,2,0,1:T(8,128)S(1)}) %tuple.76, (s32[]{:T(128)}, s32[]{:T(128)}, ...), branch_computations={%region_5.5_spmd, %region_6.8_spmd} | conditional | flops 289018368 | bytes 15974440 | solution.py:119
  207.8 2.0 fusion.21
  210.9 5.6 %conditional.4 = ((f32[2,1,512]{2,0,1:T(2,128)S(1)}, f32[2,1,512]{2,0,1:T(2,128)S(1)}, f32[2,1,64,512]{3,2,0,1:T(8,128)S(1)})) conditional(s32[]{:T(128)} %convert_element_type.118, (f32[2,1,512]{2,0,1:T(2,128)S(1)}, f32[2,1,512]{2,0,1:T(2,128)S(1)}, f32[2,1,64,512]{3,2,0,1:T(8,128)S(1)}) %tuple.74, (s32[]{:T(128)}, s32[]{:T(128)}, ...), branch_computations={%region_1.0_spmd, %region_2.4_spmd} | conditional | flops 289018368 | bytes 15974440 | solution.py:119
  214.5 2.0 fusion.1
  216.5 5.6 %conditional.5 = ((f32[2,1,512]{2,0,1:T(2,128)S(1)}, f32[2,1,512]{2,0,1:T(2,128)S(1)}, f32[2,1,64,512]{3,2,0,1:T(8,128)S(1)})) conditional(s32[]{:T(128)} %convert_element_type.119, (f32[2,1,512]{2,0,1:T(2,128)S(1)}, f32[2,1,512]{2,0,1:T(2,128)S(1)}, f32[2,1,64,512]{3,2,0,1:T(8,128)S(1)}) %tuple.76, (s32[]{:T(128)}, s32[]{:T(128)}, ...), branch_computations={%region_5.5_spmd, %region_6.8_spmd} | conditional | flops 289018368 | bytes 15974440 | solution.py:119
  220.2 2.0 fusion.21
  223.3 5.6 %conditional.4 = ((f32[2,1,512]{2,0,1:T(2,128)S(1)}, f32[2,1,512]{2,0,1:T(2,128)S(1)}, f32[2,1,64,512]{3,2,0,1:T(8,128)S(1)})) conditional(s32[]{:T(128)} %convert_element_type.118, (f32[2,1,512]{2,0,1:T(2,128)S(1)}, f32[2,1,512]{2,0,1:T(2,128)S(1)}, f32[2,1,64,512]{3,2,0,1:T(8,128)S(1)}) %tuple.74, (s32[]{:T(128)}, s32[]{:T(128)}, ...), branch_computations={%region_1.0_spmd, %region_2.4_spmd} | conditional | flops 289018368 | bytes 15974440 | solution.py:119
  226.9 2.0 fusion.1
  228.9 5.6 %conditional.5 = ((f32[2,1,512]{2,0,1:T(2,128)S(1)}, f32[2,1,512]{2,0,1:T(2,128)S(1)}, f32[2,1,64,512]{3,2,0,1:T(8,128)S(1)})) conditional(s32[]{:T(128)} %convert_element_type.119, (f32[2,1,512]{2,0,1:T(2,128)S(1)}, f32[2,1,512]{2,0,1:T(2,128)S(1)}, f32[2,1,64,512]{3,2,0,1:T(8,128)S(1)}) %tuple.76, (s32[]{:T(128)}, s32[]{:T(128)}, ...), branch_computations={%region_5.5_spmd, %region_6.8_spmd} | conditional | flops 289018368 | bytes 15974440 | solution.py:119
  232.5 2.0 fusion.21
  235.7 5.6 %conditional.4 = ((f32[2,1,512]{2,0,1:T(2,128)S(1)}, f32[2,1,512]{2,0,1:T(2,128)S(1)}, f32[2,1,64,512]{3,2,0,1:T(8,128)S(1)})) conditional(s32[]{:T(128)} %convert_element_type.118, (f32[2,1,512]{2,0,1:T(2,128)S(1)}, f32[2,1,512]{2,0,1:T(2,128)S(1)}, f32[2,1,64,512]{3,2,0,1:T(8,128)S(1)}) %tuple.74, (s32[]{:T(128)}, s32[]{:T(128)}, ...), branch_computations={%region_1.0_spmd, %region_2.4_spmd} | conditional | flops 289018368 | bytes 15974440 | solution.py:119
  239.3 2.0 fusion.1
  241.3 5.6 %conditional.5 = ((f32[2,1,512]{2,0,1:T(2,128)S(1)}, f32[2,1,512]{2,0,1:T(2,128)S(1)}, f32[2,1,64,512]{3,2,0,1:T(8,128)S(1)})) conditional(s32[]{:T(128)} %convert_element_type.119, (f32[2,1,512]{2,0,1:T(2,128)S(1)}, f32[2,1,512]{2,0,1:T(2,128)S(1)}, f32[2,1,64,512]{3,2,0,1:T(8,128)S(1)}) %tuple.76, (s32[]{:T(128)}, s32[]{:T(128)}, ...), branch_computations={%region_5.5_spmd, %region_6.8_spmd} | conditional | flops 289018368 | bytes 15974440 | solution.py:119
  244.9 2.0 fusion.21
  248.0 5.6 %conditional.4 = ((f32[2,1,512]{2,0,1:T(2,128)S(1)}, f32[2,1,512]{2,0,1:T(2,128)S(1)}, f32[2,1,64,512]{3,2,0,1:T(8,128)S(1)})) conditional(s32[]{:T(128)} %convert_element_type.118, (f32[2,1,512]{2,0,1:T(2,128)S(1)}, f32[2,1,512]{2,0,1:T(2,128)S(1)}, f32[2,1,64,512]{3,2,0,1:T(8,128)S(1)}) %tuple.74, (s32[]{:T(128)}, s32[]{:T(128)}, ...), branch_computations={%region_1.0_spmd, %region_2.4_spmd} | conditional | flops 289018368 | bytes 15974440 | solution.py:119
  251.6 2.0 fusion.1
  254.8 5.6 %conditional.4 = ((f32[2,1,512]{2,0,1:T(2,128)S(1)}, f32[2,1,512]{2,0,1:T(2,128)S(1)}, f32[2,1,64,512]{3,2,0,1:T(8,128)S(1)})) conditional(s32[]{:T(128)} %convert_element_type.118, (f32[2,1,512]{2,0,1:T(2,128)S(1)}, f32[2,1,512]{2,0,1:T(2,128)S(1)}, f32[2,1,64,512]{3,2,0,1:T(8,128)S(1)}) %tuple.74, (s32[]{:T(128)}, s32[]{:T(128)}, ...), branch_computations={%region_1.0_spmd, %region_2.4_spmd} | conditional | flops 289018368 | bytes 15974440 | solution.py:119
  261.5 5.6 %conditional.4 = ((f32[2,1,512]{2,0,1:T(2,128)S(1)}, f32[2,1,512]{2,0,1:T(2,128)S(1)}, f32[2,1,64,512]{3,2,0,1:T(8,128)S(1)})) conditional(s32[]{:T(128)} %convert_element_type.118, (f32[2,1,512]{2,0,1:T(2,128)S(1)}, f32[2,1,512]{2,0,1:T(2,128)S(1)}, f32[2,1,64,512]{3,2,0,1:T(8,128)S(1)}) %tuple.74, (s32[]{:T(128)}, s32[]{:T(128)}, ...), branch_computations={%region_1.0_spmd, %region_2.4_spmd} | conditional | flops 289018368 | bytes 15974440 | solution.py:119
  265.1 2.0 fusion.1
  268.3 5.6 %conditional.4 = ((f32[2,1,512]{2,0,1:T(2,128)S(1)}, f32[2,1,512]{2,0,1:T(2,128)S(1)}, f32[2,1,64,512]{3,2,0,1:T(8,128)S(1)})) conditional(s32[]{:T(128)} %convert_element_type.118, (f32[2,1,512]{2,0,1:T(2,128)S(1)}, f32[2,1,512]{2,0,1:T(2,128)S(1)}, f32[2,1,64,512]{3,2,0,1:T(8,128)S(1)}) %tuple.74, (s32[]{:T(128)}, s32[]{:T(128)}, ...), branch_computations={%region_1.0_spmd, %region_2.4_spmd} | conditional | flops 289018368 | bytes 15974440 | solution.py:119
  271.9 2.0 fusion.1
  275.1 5.6 %conditional.4 = ((f32[2,1,512]{2,0,1:T(2,128)S(1)}, f32[2,1,512]{2,0,1:T(2,128)S(1)}, f32[2,1,64,512]{3,2,0,1:T(8,128)S(1)})) conditional(s32[]{:T(128)} %convert_element_type.118, (f32[2,1,512]{2,0,1:T(2,128)S(1)}, f32[2,1,512]{2,0,1:T(2,128)S(1)}, f32[2,1,64,512]{3,2,0,1:T(8,128)S(1)}) %tuple.74, (s32[]{:T(128)}, s32[]{:T(128)}, ...), branch_computations={%region_1.0_spmd, %region_2.4_spmd} | conditional | flops 289018368 | bytes 15974440 | solution.py:119
  281.8 5.6 %conditional.4 = ((f32[2,1,512]{2,0,1:T(2,128)S(1)}, f32[2,1,512]{2,0,1:T(2,128)S(1)}, f32[2,1,64,512]{3,2,0,1:T(8,128)S(1)})) conditional(s32[]{:T(128)} %convert_element_type.118, (f32[2,1,512]{2,0,1:T(2,128)S(1)}, f32[2,1,512]{2,0,1:T(2,128)S(1)}, f32[2,1,64,512]{3,2,0,1:T(8,128)S(1)}) %tuple.74, (s32[]{:T(128)}, s32[]{:T(128)}, ...), branch_computations={%region_1.0_spmd, %region_2.4_spmd} | conditional | flops 289018368 | bytes 15974440 | solution.py:119
  285.4 2.0 fusion.1
  288.6 5.6 %conditional.4 = ((f32[2,1,512]{2,0,1:T(2,128)S(1)}, f32[2,1,512]{2,0,1:T(2,128)S(1)}, f32[2,1,64,512]{3,2,0,1:T(8,128)S(1)})) conditional(s32[]{:T(128)} %convert_element_type.118, (f32[2,1,512]{2,0,1:T(2,128)S(1)}, f32[2,1,512]{2,0,1:T(2,128)S(1)}, f32[2,1,64,512]{3,2,0,1:T(8,128)S(1)}) %tuple.74, (s32[]{:T(128)}, s32[]{:T(128)}, ...), branch_computations={%region_1.0_spmd, %region_2.4_spmd} | conditional | flops 289018368 | bytes 15974440 | solution.py:119
  292.2 2.0 fusion.1
  295.3 5.6 %conditional.4 = ((f32[2,1,512]{2,0,1:T(2,128)S(1)}, f32[2,1,512]{2,0,1:T(2,128)S(1)}, f32[2,1,64,512]{3,2,0,1:T(8,128)S(1)})) conditional(s32[]{:T(128)} %convert_element_type.118, (f32[2,1,512]{2,0,1:T(2,128)S(1)}, f32[2,1,512]{2,0,1:T(2,128)S(1)}, f32[2,1,64,512]{3,2,0,1:T(8,128)S(1)}) %tuple.74, (s32[]{:T(128)}, s32[]{:T(128)}, ...), branch_computations={%region_1.0_spmd, %region_2.4_spmd} | conditional | flops 289018368 | bytes 15974440 | solution.py:119
  302.1 5.6 %conditional.4 = ((f32[2,1,512]{2,0,1:T(2,128)S(1)}, f32[2,1,512]{2,0,1:T(2,128)S(1)}, f32[2,1,64,512]{3,2,0,1:T(8,128)S(1)})) conditional(s32[]{:T(128)} %convert_element_type.118, (f32[2,1,512]{2,0,1:T(2,128)S(1)}, f32[2,1,512]{2,0,1:T(2,128)S(1)}, f32[2,1,64,512]{3,2,0,1:T(8,128)S(1)}) %tuple.74, (s32[]{:T(128)}, s32[]{:T(128)}, ...), branch_computations={%region_1.0_spmd, %region_2.4_spmd} | conditional | flops 289018368 | bytes 15974440 | solution.py:119
  312.9 3.9 %collective-permute-done.4 = bf16[2,1,64,512]{3,2,0,1:T(8,128)(2,1)S(1)} collective-permute-done((bf16[2,1,64,512]{3,2,0,1:T(8,128)(2,1)S(1)}, bf16[2,1,64,512]{3,2,0,1:T(8,128)(2,1)S(1)}, u32[]{:S(2)}, u32[]{:S(2)}) %collective-permute-start.4) | collective-permute-done | bytes 131104 | tf_op jit(solution)/shard_map/ppermute | solution.py:14
  316.7 3.0 collective-permute-start.5
  319.7 2.2 reshape.161
  321.9 5.3 %all-to-all-start.1 = ((bf16[16,10,2048]{2,1,0:T(8,128)(2,1)}), bf16[16,10,2048]{2,1,0:T(8,128)(2,1)S(1)}, u32[]{:S(2)}, u32[]{:S(2)}) async-start(bf16[16,10,2048]{2,1,0:T(8,128)(2,1)} %reshape.161), calls=%async_computation.2 | async-start | bytes 2097152 | tf_op jit(solution)/shard_map/all_to_all | solution.py:195
  328.2 14.6 %collective-permute-done.6 = bf16[2,1,64,512]{3,2,0,1:T(8,128)(2,1)S(1)} collective-permute-done((bf16[2,1,64,512]{3,2,0,1:T(8,128)(2,1)S(1)}, bf16[2,1,64,512]{3,2,0,1:T(8,128)(2,1)S(1)}, u32[]{:S(2)}, u32[]{:S(2)}) %collective-permute-start.6) | collective-permute-done | bytes 131104 | tf_op jit(solution)/shard_map/ppermute | solution.py:14
  342.8 6.4 %collective-permute-done.7 = bf16[2,1,64,512]{3,2,0,1:T(8,128)(2,1)S(1)} collective-permute-done((bf16[2,1,64,512]{3,2,0,1:T(8,128)(2,1)S(1)}, bf16[2,1,64,512]{3,2,0,1:T(8,128)(2,1)S(1)}, u32[]{:S(2)}, u32[]{:S(2)}) %collective-permute-start.7) | collective-permute-done | bytes 131104 | tf_op jit(solution)/shard_map/ppermute | solution.py:14
  (251 shorter events, 108.4 us)
Async XLA Ops:
  7.2 112.8 %copy-start = (bf16[2,128,2048]{2,1,0:T(8,128)(2,1)S(1)}, bf16[2,128,2048]{2,1,0:T(8,128)(2,1)}, u32[]{:S(2)}) copy-start(bf16[2,128,2048]{2,1,0:T(8,128)(2,1)} %param.29) | copy-start | bytes 3145732
  7.2 104.2 %all-gather.5.cloned.1.call-start = ((), (), s32[]{:S(2)}) async-start(), calls=%async_computation.4 | async-start | bytes 11837440 | tf_op jit(solution)/shard_map/all_gather | solution.py:23
  15.3 26.3 %copy-start.3 = (bf16[2,64,1024]{2,1,0:T(8,128)(2,1)S(1)}, bf16[2,64,1024]{2,1,0:T(8,128)(2,1)}, u32[]{:S(2)}) copy-start(bf16[2,64,1024]{2,1,0:T(8,128)(2,1)} %param.20) | copy-start | bytes 786436
  41.5 71.3 %copy-start.5 = (bf16[2,128,2048]{2,1,0:T(8,128)(2,1)S(1)}, bf16[2,128,2048]{2,1,0:T(8,128)(2,1)}, u32[]{:S(2)}) copy-start(bf16[2,128,2048]{2,1,0:T(8,128)(2,1)} %param.27) | copy-start | bytes 3145732
  41.5 150.0 %all-gather.3.cloned.1.call-start = ((), (), s32[]{:S(2)}) async-start(), calls=%async_computation.3 | async-start | bytes 8912896 | tf_op jit(solution)/shard_map/all_gather | solution.py:23
  43.5 276.2 %reduce-scatter.2.cloned.1.call-start = ((), (), s32[]{:S(2)}) async-start(), calls=%async_computation.5 | async-start | bytes 11141120 | tf_op jit(solution)/shard_map/reduce_scatter | solution.py:187
  136.4 1.0 copy-start.2
  136.4 14.0 %copy-start.4 = (f32[2,1,16384]{2,1,0:T(1,128)S(1)}, f32[2,1,16384]{2,1,0:T(1,128)}, u32[]{:S(2)}) copy-start(f32[2,1,16384]{2,1,0:T(1,128)} %param.21) | copy-start | bytes 393220
  137.4 5.7 %collective-permute-start = (bf16[2,1,64,512]{3,2,0,1:T(8,128)(2,1)S(1)}, bf16[2,1,64,512]{3,2,0,1:T(8,128)(2,1)S(1)}, u32[]{:S(2)}, u32[]{:S(2)}) collective-permute-start(bf16[2,1,64,512]{3,2,0,1:T(8,128)(2,1)S(1)} %get-tuple-element.655), channel_id=1, source_target_pairs={{0,16},{16,0},{32,48},{48,32},{64,80},{80,64},{96,112},{112,96},{1... | collective-permute-start | bytes 393224 | tf_op jit(solution)/shard_map/ppermute | solution.py:14
  143.1 6.5 %collective-permute-start.1 = (bf16[2,1,64,512]{3,2,0,1:T(8,128)(2,1)S(1)}, bf16[2,1,64,512]{3,2,0,1:T(8,128)(2,1)S(1)}, u32[]{:S(2)}, u32[]{:S(2)}) collective-permute-start(bf16[2,1,64,512]{3,2,0,1:T(8,128)(2,1)S(1)} %collective-permute-done), channel_id=1, source_target_pairs={{0,32},{16,48},{32,0},{48,16},{64,96},{80,112},{96,64},{112,80},{1... | collective-permute-start | bytes 393224 | tf_op jit(solution)/shard_map/ppermute | solution.py:14
  149.6 7.8 %collective-permute-start.2 = (bf16[2,1,64,512]{3,2,0,1:T(8,128)(2,1)S(1)}, bf16[2,1,64,512]{3,2,0,1:T(8,128)(2,1)S(1)}, u32[]{:S(2)}, u32[]{:S(2)}) collective-permute-start(bf16[2,1,64,512]{3,2,0,1:T(8,128)(2,1)S(1)} %collective-permute-done.1), channel_id=1, source_target_pairs={{0,64},{16,80},{32,96},{48,112},{64,0},{80,16},{96,32},{112,48},{1... | collective-permute-start | bytes 393224 | tf_op jit(solution)/shard_map/ppermute | solution.py:14
  157.4 40.0 %collective-permute-start.3 = (bf16[2,1,64,512]{3,2,0,1:T(8,128)(2,1)S(1)}, bf16[2,1,64,512]{3,2,0,1:T(8,128)(2,1)S(1)}, u32[]{:S(2)}, u32[]{:S(2)}) collective-permute-start(bf16[2,1,64,512]{3,2,0,1:T(8,128)(2,1)S(1)} %collective-permute-done.2), channel_id=1, source_target_pairs={{0,128},{16,144},{32,160},{48,176},{64,192},{80,208},{96,224},{112... | collective-permute-start | bytes 393224 | tf_op jit(solution)/shard_map/ppermute | solution.py:14
  311.2 40.1 %copy-start.1 = (bf16[2,128,2048]{2,1,0:T(8,128)(2,1)S(1)}, bf16[2,128,2048]{2,1,0:T(8,128)(2,1)}, u32[]{:S(2)}) copy-start(bf16[2,128,2048]{2,1,0:T(8,128)(2,1)} %param.29) | copy-start | bytes 3145732
  311.3 5.5 %collective-permute-start.4 = (bf16[2,1,64,512]{3,2,0,1:T(8,128)(2,1)S(1)}, bf16[2,1,64,512]{3,2,0,1:T(8,128)(2,1)S(1)}, u32[]{:S(2)}, u32[]{:S(2)}) collective-permute-start(bf16[2,1,64,512]{3,2,0,1:T(8,128)(2,1)S(1)} %divide_convert_fusion), channel_id=1, source_target_pairs={{0,16},{16,0},{32,48},{48,32},{64,80},{80,64},{96,112},{112,96},{1... | collective-permute-start | bytes 393224 | tf_op jit(solution)/shard_map/ppermute | solution.py:14
  316.7 10.5 %collective-permute-start.5 = (bf16[2,1,64,512]{3,2,0,1:T(8,128)(2,1)S(1)}, bf16[2,1,64,512]{3,2,0,1:T(8,128)(2,1)S(1)}, u32[]{:S(2)}, u32[]{:S(2)}) collective-permute-start(bf16[2,1,64,512]{3,2,0,1:T(8,128)(2,1)S(1)} %collective-permute-done.4), channel_id=1, source_target_pairs={{0,32},{16,48},{32,0},{48,16},{64,96},{80,112},{96,64},{112,80},{1... | collective-permute-start | bytes 393224 | tf_op jit(solution)/shard_map/ppermute | solution.py:14
  321.9 28.1 %all-to-all-start.1 = ((bf16[16,10,2048]{2,1,0:T(8,128)(2,1)}), bf16[16,10,2048]{2,1,0:T(8,128)(2,1)S(1)}, u32[]{:S(2)}, u32[]{:S(2)}) async-start(bf16[16,10,2048]{2,1,0:T(8,128)(2,1)} %reshape.161), calls=%async_computation.2 | async-start | bytes 2097152 | tf_op jit(solution)/shard_map/all_to_all | solution.py:195
  327.2 15.5 %collective-permute-start.6 = (bf16[2,1,64,512]{3,2,0,1:T(8,128)(2,1)S(1)}, bf16[2,1,64,512]{3,2,0,1:T(8,128)(2,1)S(1)}, u32[]{:S(2)}, u32[]{:S(2)}) collective-permute-start(bf16[2,1,64,512]{3,2,0,1:T(8,128)(2,1)S(1)} %collective-permute-done.5), channel_id=1, source_target_pairs={{0,64},{16,80},{32,96},{48,112},{64,0},{80,16},{96,32},{112,48},{1... | collective-permute-start | bytes 393224 | tf_op jit(solution)/shard_map/ppermute | solution.py:14
  342.7 6.5 %collective-permute-start.7 = (bf16[2,1,64,512]{3,2,0,1:T(8,128)(2,1)S(1)}, bf16[2,1,64,512]{3,2,0,1:T(8,128)(2,1)S(1)}, u32[]{:S(2)}, u32[]{:S(2)}) collective-permute-start(bf16[2,1,64,512]{3,2,0,1:T(8,128)(2,1)S(1)} %collective-permute-done.6), channel_id=1, source_target_pairs={{0,128},{16,144},{32,160},{48,176},{64,192},{80,208},{96,224},{112... | collective-permute-start | bytes 393224 | tf_op jit(solution)/shard_map/ppermute | solution.py:14
Sparse Core Ops, SparseCore 0:
  41.7 69.6 all-gather.4
  114.4 77.1 all-gather.2
  194.1 75.0 reduce-scatter.1
where the time goes:
time: 359 us; the launch traced here: 358 us
  waiting for transfers between devices  140 us (39%)
  matrix products  80.9 us (23%)
  other arithmetic  49.9 us (14%)
  local copies, waits for them, and re-layouts  29.9 us (8%)
  blocking collectives  23 us (6%)
  starting transfers between devices  17.6 us (5%)
  between operations  14 us (4%)
    all_gather x2, waiting for transfers between devices, sent_together(): lax.all_gather(both, axis, axis=dim, tiled=True)  101 us
    ppermute x8, waiting for transfers between devices, partner(): lax.ppermute(x, axis, [(i, i ^ 1 << distance) for i in range(lax.axis_siz...  39.4 us
    reduce_sum x17, other arithmetic, absorb(): total_new = total_old * shrink + jnp.sum(weights, axis=3)  33.3 us
    dot_general x17, matrix products, absorb(): jnp.einsum('shqk,shdk->shdq', weights.astype(jnp.bfloat16), value_block,...  29 us
    dot_general x17, matrix products, absorb(): jnp.einsum('shdq,shdk->shqk', query_block, key_block, preferred_element_t...  25 us
    all_to_all x1, blocking collectives, side_by_side(): lax.all_to_all(both, axis, split_axis=split_dim, concat_axis=concat_dim,...  23 us
    reshape x16, local copies, waits for them, and re-layouts, visit_block(): lax.dynamic_slice_in_dim(value_piece, offset, key_span, 2)  17.2 us
    dot_general x1, matrix products, mixture(): jnp.einsum('ref,efd->rd', hidden, down_weight, preferred_element_type=jnp...  16.4 us
  transfers between devices with their start and end apart: 12, of which 8 were waited for; matrix products, arithmetic and copies ran while one was open for 41% of the time, Pallas kernels for 0%

commit v1 on v0

v1 whole, which is shorter than its diff:
```python
import jax
import jax.numpy as jnp
from jax import lax
from jax.experimental import pallas as pl
from jax.experimental.pallas import tpu as pltpu
from jax.sharding import PartitionSpec as P

MESH = pl.DeviceIdType.MESH
F32 = jnp.float32
BF16 = jnp.bfloat16

NX, NY, NZ = 4, 4, 8
NEP = NX * NY
SEG = 1024
HEAD = 64
TOK = 128
DIM = 2048
CAP = 10
QB = 8
CW = DIM // QB
HALF = 8 * CAP
STACK = QB * HALF
PAGE = QB * CAP
RT = 16
NEG = -1e30
EPS = 1e-6
ACC = 80


def dot(a, b, ca=1, cb=0):
    return lax.dot_general(a, b, (((ca,), (cb,)), ((), ())), preferred_element_type=F32)


def iota(shape, dim):
    return lax.broadcasted_iota(jnp.int32, shape, dim)


def iota_f(shape, dim):
    return iota(shape, dim).astype(F32)


def onehot(cond):
    return jnp.where(cond, 1.0, 0.0).astype(BF16)


def rem(a, n):
    return lax.rem(a, jnp.int32(n))


def div(a, n):
    return lax.div(a, jnp.int32(n))


def stacked_of_paged(r):
    src = jnp.floor((r + 0.5) * (1.0 / PAGE))
    left = r - PAGE * src
    blk = jnp.floor((left + 0.5) * (1.0 / CAP))
    slot = left - CAP * blk
    return HALF * blk + CAP * src + slot


def body(
    q_hbm, k_hbm, v_hbm, gate_ref, x_ref, gain_ref, small_ref, wg_hbm, wu_hbm, wd_hbm,
    att_ref, out_ref,
    wg, wu, wd, pages, arr, retp, ret, perm_in, perm_out, mh, pt,
    gown, gsib, pown, tosib, sibr, rsr, kraw, vaug, qaug, kt, acc, orecv,
    w_sem, l_sem, a_s, a_r, b_s, b_r, ag_s, ag_r, dr_s, dr_r, dp_s, dp_r, rs_s, rs_r,
    t_s, t_r, o_s, o_r,
):
    ep = lax.axis_index("ep")
    tp = lax.axis_index("tp")
    y, x = div(ep, NX), rem(ep, NX)
    z, core = div(tp, 2), rem(tp, 2)
    sib = z * 2 + (1 - core)
    up = rem(z + 1, NZ) * 2 + core
    down = rem(z + NZ - 1, NZ) * 2 + core
    ring = (up, down)

    def remote(src, dst, ss, rs, e, t):
        return pltpu.make_async_remote_copy(
            src_ref=src, dst_ref=dst, send_sem=ss, recv_sem=rs,
            device_id=(e, t), device_id_type=MESH,
        )

    barrier = pltpu.get_barrier_semaphore()

    @pl.loop(1, NEP)
    def _(d):
        pl.semaphore_signal(barrier, inc=1, device_id=(rem(ep + d, NEP), tp), device_id_type=MESH)

    for t in (up, down, sib):
        pl.semaphore_signal(barrier, inc=1, device_id=(ep, t), device_id_type=MESH)

    w_copies = [
        pltpu.make_async_copy(src, dst, w_sem.at[n])
        for n, (src, dst) in enumerate(((wg_hbm, wg), (wu_hbm, wu), (wd_hbm, wd)))
    ]
    for c in w_copies:
        c.start()
    q_own = (y, 4 + x)
    kv_own = (x, 4 + y)
    l_copies = []
    for s in range(2):
        l_copies += [
            pltpu.make_async_copy(q_hbm.at[s], qaug.at[q_own[s], pl.ds(0, HEAD)], l_sem.at[3 * s]),
            pltpu.make_async_copy(k_hbm.at[s], kraw.at[kv_own[s]], l_sem.at[3 * s + 1]),
            pltpu.make_async_copy(v_hbm.at[s], vaug.at[kv_own[s], pl.ds(0, HEAD)], l_sem.at[3 * s + 2]),
        ]
    for c in l_copies:
        c.start()

    tok = x_ref[...].astype(F32)
    normed = (
        tok * lax.rsqrt(jnp.mean(tok * tok, axis=1, keepdims=True) + EPS) * gain_ref[...]
    ).astype(BF16)
    l0, l1 = small_ref[0:1, :], small_ref[1:2, :]
    gw, gc = small_ref[2:3, :], small_ref[3:4, :]
    top = jnp.maximum(l0, l1)
    e0, e1 = jnp.exp(l0 - top), jnp.exp(l1 - top)
    r0 = (gw * (e0 / (e0 + e1))).astype(BF16).astype(F32)
    r1 = (gw * (e1 / (e0 + e1))).astype(BF16).astype(F32)
    member = jnp.where(iota_f((NEP, TOK), 0) == gc, 1.0, 0.0)
    earlier = onehot(iota((TOK, TOK), 0) < iota((TOK, TOK), 1))
    before = dot(member.astype(BF16), earlier)
    slot = jnp.sum(before * member, axis=0, keepdims=True)
    flat = gc * PAGE + slot
    rows_p = iota_f((NEP * PAGE, TOK), 0)
    packed = jnp.zeros((NEP * PAGE, CW), F32)
    for b in range(0, QB, 2):
        put = jnp.concatenate(
            [onehot(rows_p == flat + CAP * b), onehot(rows_p == flat + CAP * (b + 1))], axis=1
        )
        cols = jnp.concatenate(
            [normed[:, b * CW:(b + 1) * CW], normed[:, (b + 1) * CW:(b + 2) * CW]], axis=0
        )
        packed = packed + dot(put, cols)
    packed = packed.astype(BF16)
    eye = iota((TOK, TOK), 0) == iota((TOK, TOK), 1)
    ones = jnp.ones((TOK, TOK), BF16)
    col_g = dot(jnp.where(eye, gc, 0.0).astype(BF16), ones)
    col_s = dot(jnp.where(eye, slot, 0.0).astype(BF16), ones)
    flat10 = col_g * CAP + col_s
    place10 = onehot(iota_f((TOK, CW), 1) == jnp.concatenate([flat10, flat10], axis=1))
    e_rows = iota((RT, TOK), 0)
    rr = jnp.where(e_rows == 0, r0, jnp.where(e_rows == 1, r1, 0.0)).astype(BF16)
    rt_all = dot(rr, place10).astype(BF16)
    for g in range(NEP):
        pages[g, 0:PAGE, :] = packed[g * PAGE:(g + 1) * PAGE, :]
        pages[g, PAGE:PAGE + RT, :] = rt_all

    pl.semaphore_wait(barrier, NEP + 2)

    def a2a(e):
        return remote(pages.at[e], arr.at[ep], a_s.at[e], a_r.at[ep], e, tp)

    @pl.loop(1, NEP)
    def _(d):
        a2a(rem(ep + d, NEP)).start()

    arr[ep] = pages[ep]

    def along(axis, d):
        if axis == 0:
            return y * NX + rem(x + d, NX)
        return rem(y + d, NY) * NX + x

    def spread(s, d):
        kv_axis, q_axis = s, 1 - s
        e_kv, e_q = along(kv_axis, d), along(q_axis, d)
        return (
            remote(k_hbm.at[s], kraw.at[kv_own[s]], t_s.at[s, 0, d], t_r.at[0, kv_own[s]], e_kv, tp),
            remote(v_hbm.at[s], vaug.at[kv_own[s], pl.ds(0, HEAD)], t_s.at[s, 1, d],
                   t_r.at[1, kv_own[s]], e_kv, tp),
            remote(q_hbm.at[s], qaug.at[q_own[s], pl.ds(0, HEAD)], t_s.at[s, 2, d],
                   t_r.at[2, q_own[s]], e_q, tp),
        )

    for s in range(2):
        for d in range(1, 4):
            for c in spread(s, d):
                c.start()

    sq = (STACK, STACK)
    perm_in[...] = onehot(iota_f(sq, 0) == stacked_of_paged(iota_f(sq, 1)))
    perm_out[...] = onehot(iota_f(sq, 1) == stacked_of_paged(iota_f(sq, 0)))
    epf = ep.astype(F32)
    for sl in range(8):
        off = iota_f((CW, CW), 0) - CAP * epf
        hit = (iota_f((CW, CW), 1) - CAP * sl == off) & (off >= 0.0) & (off < CAP)
        mh[sl * CW:(sl + 1) * CW, :] = onehot(hit)
    col_flat = col_g * PAGE + col_s
    wide = jnp.concatenate([col_flat] * (NEP * PAGE // TOK), axis=1)
    lanes_p = iota_f((TOK, NEP * PAGE), 1)
    for b in range(QB):
        pt[b * TOK:(b + 1) * TOK, :] = onehot(lanes_p == wide + CAP * b)

    @pl.loop(0, 8)
    def _(n):
        qaug[n, HEAD:2 * HEAD, :] = onehot(iota((HEAD, SEG), 0) < 3)
        vaug[n, HEAD:ACC, :] = onehot(iota((ACC - HEAD, SEG), 0) < 1)
        acc[n, 0:72, :] = jnp.zeros((72, SEG), F32)
        acc[n, 72:ACC, :] = jnp.full((ACC - 72, SEG), NEG, F32)

    for h in range(2):
        rsr[h, 0] = jnp.zeros((STACK, CW), BF16)

    def ag(h, i):
        return remote(gown.at[h, i], gown.at[h, i + 1], ag_s.at[h, i], ag_r.at[h, i], ep, ring[h])

    def rows_to_sib(h, j):
        return remote(gown.at[h, j], gsib.at[h, j], dr_s.at[h, j], dr_r.at[h, j], ep, sib)

    def sums_to_sib(h, j):
        return remote(tosib.at[h, j], sibr.at[h, j], dp_s.at[h, j], dp_r.at[h, j], ep, sib)

    def rs(h, r):
        return remote(pown.at[h, r + 1], rsr.at[h, r + 1], rs_s.at[h, r], rs_r.at[h, r], ep, ring[h])

    for h in range(2):
        for sl in range(8):
            src = 8 * h + sl

            @pl.when(src != ep)
            def _():
                remote(pages.at[src], arr.at[src], a_s.at[src], a_r.at[src], src, tp).wait_recv()

        paged = jnp.concatenate([arr[8 * h + sl, 0:PAGE, :] for sl in range(8)], axis=0)
        rts = jnp.concatenate([arr[8 * h + sl, PAGE:PAGE + RT, :] for sl in range(8)], axis=1)
        gown[h, 0, 0:STACK, :] = dot(perm_in[...], paged).astype(BF16)
        gown[h, 0, STACK:STACK + RT, :] = dot(rts, mh[...]).astype(BF16)
        ag(h, 0).start()
        rows_to_sib(h, 0).start()

    for c in w_copies:
        c.wait()
    for c in l_copies:
        c.wait()

    def expert(i):
        j = rem(i + 1, NZ)
        pieces = (gown.at[0, j], gown.at[1, j], gsib.at[0, i], gsib.at[1, i])
        lhs = jnp.concatenate(
            [
                jnp.concatenate([p[b * HALF:(b + 1) * HALF, :] for b in range(QB)], axis=1)
                for p in pieces
            ],
            axis=0,
        )
        diag = iota((HALF, TOK), 0) == iota((HALF, TOK), 1)
        one = jnp.ones((TOK, TOK), BF16)
        scale = []
        for p in pieces:
            tile = p[STACK:STACK + RT, 0:TOK].astype(F32)
            scale.append(
                jnp.concatenate(
                    [dot(jnp.where(diag, tile[e:e + 1, :], 0.0).astype(BF16), one) for e in range(2)],
                    axis=1,
                )
            )
        scale = jnp.concatenate(scale, axis=0)
        gate = dot(lhs, wg[...], 1, 1)
        upv = dot(lhs, wu[...], 1, 1)
        hidden = (gate / (1.0 + jnp.exp(-gate)) * upv * scale).astype(BF16)
        outs = (pown.at[0, j], pown.at[1, j], tosib.at[0, i], tosib.at[1, i])
        for b in range(QB):
            prod = dot(hidden, wd[:, b * CW:(b + 1) * CW]).astype(BF16)
            for n, o in enumerate(outs):
                o[b * HALF:(b + 1) * HALF, :] = prod[n * HALF:(n + 1) * HALF, :]
        for h in range(2):
            sums_to_sib(h, i).start()

    def attention_ready():
        for s in range(2):
            for d in range(1, 4):
                kv = 4 * s + rem(kv_own[s] - 4 * s + d, 4)
                qs = 4 * s + rem(q_own[s] - 4 * s + d, 4)
                remote(k_hbm.at[s], kraw.at[kv], t_s.at[s, 0, d], t_r.at[0, kv], ep, sib).wait_recv()
                remote(v_hbm.at[s], vaug.at[kv, pl.ds(0, HEAD)], t_s.at[s, 1, d], t_r.at[1, kv], ep,
                       sib).wait_recv()
                remote(q_hbm.at[s], qaug.at[qs, pl.ds(0, HEAD)], t_s.at[s, 2, d], t_r.at[2, qs], ep,
                       sib).wait_recv()

        @pl.loop(0, 8)
        def _(n):
            s = div(n, 4)
            chunk = (1 - s) * (4 * y + n) + s * (x + 4 * (n - 4))
            g = gate_ref[s, :, pl.ds(pl.multiple_of(chunk * SEG, SEG), SEG)]
            d = g[:, SEG - 1:SEG] - g
            hi = d.astype(BF16).astype(F32)
            mid = (d - hi).astype(BF16).astype(F32)
            lo = d - hi - mid
            r = iota((8, SEG), 0)
            rows = jnp.where(r == 0, hi, jnp.where(r == 1, mid, jnp.where(r == 2, lo, 0.0)))
            feats = kraw[n].astype(F32) * 0.125
            full = jnp.concatenate([feats, rows, jnp.zeros((56, SEG), F32)], axis=0)
            kt[n] = full.T.astype(BF16)

    n_first = 4 * (3 - y) + x + 1

    def unit(b):
        s = (b >= n_first).astype(jnp.int32)
        u0 = b
        late0 = (u0 > x).astype(jnp.int32)
        t0 = late0 * (u0 - x - 1)
        k0 = y + late0 * (1 + div(t0, 4))
        m0 = late0 * rem(t0, 4) + (1 - late0) * u0
        d0 = (u0 == x).astype(jnp.int32)
        u1 = s * (b - n_first)
        late1 = (u1 >= 4 * y).astype(jnp.int32)
        k1 = late1 * y + (1 - late1) * div(u1, 4)
        m1 = late1 * (x + u1 - 4 * y) + (1 - late1) * rem(u1, 4)
        d1 = (u1 == 4 * y).astype(jnp.int32)
        qs = (1 - s) * k0 + s * (4 + m1)
        kv = (1 - s) * m0 + s * (4 + k1)
        qc = (1 - s) * (4 * k0 + x) + s * (4 * y + m1)
        kc = (1 - s) * (4 * y + m0) + s * (x + 4 * k1)
        slack = (1 - ((1 - s) * d0 + s * d1)) * (2 * SEG)
        qs, kv = rem(qs, 8), rem(kv, 8)
        qc, kc = rem(qc, NEP), rem(kc, NEP)
        ref_end = gate_ref[s, :, pl.ds(pl.multiple_of(kc * SEG + SEG - 128, 128), 128)][:, 127:128]

        @pl.loop(0, SEG // 256)
        def _(c):
            at = pl.multiple_of(c * 256, 256)
            lanes = pl.ds(at, 256)
            sc = dot(kt[kv], qaug[qs, :, lanes])
            keep = iota((SEG, 256), 0) <= iota((SEG, 256), 1) + (at + slack)
            sc = jnp.where(keep, sc, NEG)
            peak = jnp.max(sc, axis=0, keepdims=True)
            w = jnp.exp(sc - peak).astype(BF16)
            o = dot(vaug[kv], w)
            gq = gate_ref[s, :, pl.ds(pl.multiple_of(qc * SEG + at, 256), 256)]
            peak = peak + (gq - ref_end)
            old = acc[qs, 72:73, lanes]
            new = jnp.maximum(old, peak)
            acc[qs, 0:72, lanes] = acc[qs, 0:72, lanes] * jnp.exp(old - new) + o[0:72] * jnp.exp(peak - new)
            acc[qs, 72:ACC, lanes] = jnp.broadcast_to(new, (ACC - 72, 256))

    def give(s, d):
        e = along(1 - s, d)
        mine = q_own[s] - 4 * s
        theirs = 4 * s + rem(mine + d, 4)
        return remote(acc.at[theirs], orecv.at[s, mine], o_s.at[s, d], o_r.at[s, mine], e, tp)

    UNITS = 17
    PER = 4

    @pl.loop(0, NZ)
    def _(i):
        @pl.when(i < NZ - 1)
        def _():
            for h in range(2):
                ag(h, i).wait_recv()

                @pl.when(i < NZ - 2)
                def _():
                    ag(h, i + 1).start()

                rows_to_sib(h, i + 1).start()

        for h in range(2):
            rows_to_sib(h, i).wait_recv()
        expert(i)

        @pl.when(i == 1)
        def _():
            attention_ready()

        first = jnp.maximum(PER * (i - 1), 0)
        last = jnp.minimum(PER * i, UNITS)

        @pl.loop(first, last)
        def _(b):
            unit(b)

        @pl.when(i == 6)
        def _():
            for s in range(2):
                for d in range(1, 4):
                    give(s, d).start()

        @pl.when(i >= 1)
        def _():
            r = i - 1
            for h in range(2):
                sums_to_sib(h, i).wait_recv()

                @pl.when(r >= 1)
                def _():
                    rs(h, r - 1).wait_recv()

                pown[h, i] = (
                    pown[h, i].astype(F32) + sibr[h, i].astype(F32) + rsr[h, r].astype(F32)
                ).astype(BF16)
                rs(h, r).start()

    def back(e):
        return remote(retp.at[e], ret.at[ep], b_s.at[e], b_r.at[ep], e, tp)

    for h in range(2):
        sums_to_sib(h, 0).wait_recv()
        rs(h, NZ - 2).wait_recv()
        total = (
            pown[h, 0].astype(F32) + sibr[h, 0].astype(F32) + rsr[h, NZ - 1].astype(F32)
        ).astype(BF16)
        paged = dot(perm_out[...], total).astype(BF16)
        for sl in range(8):
            src = 8 * h + sl
            retp[src] = paged[sl * PAGE:(sl + 1) * PAGE, :]

            @pl.when(src != ep)
            def _():
                back(src).start()

    ret[ep] = retp[ep]

    for s in range(2):
        mine = q_own[s] - 4 * s
        for d in range(1, 4):
            slot_d = rem(mine + d, 4)
            remote(acc.at[0], orecv.at[s, slot_d], o_s.at[s, d], o_r.at[s, slot_d], ep, sib).wait_recv()
        for c in range(SEG // 256):
            lanes = slice(c * 256, (c + 1) * 256)
            parts = [acc.at[q_own[s]]] + [orecv.at[s, rem(mine + d, 4)] for d in range(1, 4)]
            peaks = [p[72:73, lanes] for p in parts]
            top = jnp.maximum(jnp.maximum(peaks[0], peaks[1]), jnp.maximum(peaks[2], peaks[3]))
            mix = sum(p[0:72, lanes] * jnp.exp(m - top) for p, m in zip(parts, peaks))
            att_ref[s, :, lanes] = (mix[0:HEAD] / mix[HEAD:HEAD + 1]).astype(BF16)

    for src in range(NEP):
        @pl.when(src != ep)
        def _():
            remote(retp.at[src], ret.at[src], b_s.at[src], b_r.at[src], src, tp).wait_recv()

    back_rows = jnp.concatenate([ret[g] for g in range(NEP)], axis=0)
    placed = dot(pt[...], back_rows).astype(BF16)
    for b in range(QB):
        out_ref[:, b * CW:(b + 1) * CW] = placed[b * TOK:(b + 1) * TOK, :]

    @pl.loop(1, NEP)
    def _(d):
        e = rem(ep + d, NEP)
        a2a(e).wait_send()
        back(e).wait_send()

    for s in range(2):
        for d in range(1, 4):
            for c in spread(s, d):
                c.wait_send()
            give(s, d).wait_send()
    for h in range(2):
        @pl.loop(0, NZ - 1)
        def _(i):
            ag(h, i).wait_send()
            rs(h, i).wait_send()

        @pl.loop(0, NZ)
        def _(i):
            rows_to_sib(h, i).wait_send()
            sums_to_sib(h, i).wait_send()


def local(
    queries, key_vectors, value_vectors, cumulative_gate, expert_input, norm_gain,
    group_choice, group_weight, expert_logits, gate_weight, up_weight, down_weight,
):
    small = jnp.concatenate(
        [expert_logits.T, group_weight[None], group_choice.astype(F32)[None], jnp.zeros((4, TOK), F32)],
        axis=0,
    )
    vmem = pl.BlockSpec(memory_space=pltpu.VMEM)
    hbm = pl.BlockSpec(memory_space=pltpu.HBM)
    dma = pltpu.SemaphoreType.DMA
    v = pltpu.VMEM
    scratch = [
        v((256, DIM), BF16), v((256, DIM), BF16), v((256, DIM), BF16),
        v((NEP, PAGE + RT, CW), BF16), v((NEP, PAGE + RT, CW), BF16),
        v((NEP, PAGE, CW), BF16), v((NEP, PAGE, CW), BF16),
        v((STACK, STACK), BF16), v((STACK, STACK), BF16),
        v((8 * CW, CW), BF16), v((QB * TOK, NEP * PAGE), BF16),
        v((2, NZ, STACK + RT, CW), BF16), v((2, NZ, STACK + RT, CW), BF16),
        v((2, NZ, STACK, CW), BF16), v((2, NZ, STACK, CW), BF16), v((2, NZ, STACK, CW), BF16),
        v((2, NZ, STACK, CW), BF16),
        v((8, HEAD, SEG), BF16), v((8, ACC, SEG), BF16), v((8, 2 * HEAD, SEG), BF16),
        v((8, SEG, 2 * HEAD), BF16), v((8, ACC, SEG), F32), v((2, 4, ACC, SEG), F32),
        dma((3,)), dma((6,)), dma((NEP,)), dma((NEP,)), dma((NEP,)), dma((NEP,)),
        dma((2, NZ - 1)), dma((2, NZ - 1)), dma((2, NZ)), dma((2, NZ)), dma((2, NZ)), dma((2, NZ)),
        dma((2, NZ - 1)), dma((2, NZ - 1)), dma((2, 3, 4)), dma((3, 8)), dma((2, 4)), dma((2, 4)),
    ]
    return pl.pallas_call(
        body,
        out_shape=(
            jax.ShapeDtypeStruct(queries.shape, BF16),
            jax.ShapeDtypeStruct(expert_input.shape, BF16),
        ),
        in_specs=[hbm, hbm, hbm, vmem, vmem, vmem, vmem, hbm, hbm, hbm],
        out_specs=(vmem, vmem),
        scratch_shapes=scratch,
        compiler_params=pltpu.CompilerParams(
            collective_id=0, has_side_effects=True, vmem_limit_bytes=67043328
        ),
    )(
        queries, key_vectors, value_vectors, cumulative_gate, expert_input, norm_gain[None],
        small, gate_weight.reshape(256, DIM), up_weight.reshape(256, DIM), down_weight.reshape(256, DIM),
    )


def solution(mesh):
    return jax.shard_map(
        local,
        mesh=mesh,
        in_specs=(
            P(None, "tp", "ep"),
            P(None, "tp", "ep"),
            P(None, "tp", "ep"),
            P(None, "tp", None),
            P(("ep", "tp"), None),
            P(),
            P(("ep", "tp")),
            P(("ep", "tp")),
            P(("ep", "tp"), None),
            P("ep", "tp", None),
            P("ep", "tp", None),
            P("ep", "tp", None),
        ),
        out_specs=(P(None, "tp", "ep"), P(("ep", "tp"), None)),
        check_vma=False,
    )
```

time: 359 us -> 158 us (0.44)
  Pallas kernels: 0 us -> 150 us
  waiting for transfers between devices: 140 us -> 0 us
  matrix products: 80.9 us -> 0 us
  other arithmetic: 49.9 us -> 0.66 us
  local copies, waits for them, and re-layouts: 29.9 us -> 3.85 us
  blocking collectives: 23 us -> 0 us
  starting transfers between devices: 17.6 us -> 0 us
  between operations: 14 us -> 0.66 us
    pallas_call x0 -> x1, Pallas kernels: none -> 150 us  [local(): pl.pallas_call(body, out_shape=(jax.ShapeDtypeStruct(queries.shape, BF16)...]
    all_gather x2 -> x0, waiting for transfers between devices: 101 us -> none  [sent_together(): lax.all_gather(both, axis, axis=dim, tiled=True)]
    dot_general x39 -> x0, matrix products: 80.9 us -> none  [the longest x17 29 us: absorb(): jnp.einsum('shqk,shdk->shdq', weights.astype(jnp.bfloat16), value_block,...]
    ppermute x8 -> x0, waiting for transfers between devices: 39.4 us -> none  [partner(): lax.ppermute(x, axis, [(i, i ^ 1 << distance) for i in range(lax.axis_siz...]
    reduce_sum x20 -> x0, other arithmetic: 36.1 us -> none  [the longest x17 33.3 us: absorb(): total_new = total_old * shrink + jnp.sum(weights, axis=3)]
    all_to_all x1 -> x0, blocking collectives: 23 us -> none  [side_by_side(): lax.all_to_all(both, axis, split_axis=split_dim, concat_axis=concat_dim,...]
    reshape x23 -> x0, local copies, waits for them, and re-layouts: 21.3 us -> none  [the longest x16 17.2 us: visit_block(): lax.dynamic_slice_in_dim(value_piece, offset, key_span, 2)]
    ppermute x8 -> x0, starting transfers between devices: 12.2 us -> none  [partner(): lax.ppermute(x, axis, [(i, i ^ 1 << distance) for i in range(lax.axis_siz...]
  transfers between devices with their start and end apart: 12 -> 0, of which waited for: 8 -> 0; matrix products, arithmetic and copies ran while one was open for 41% -> 0% of each run, Pallas kernels for 0% -> 0%
where the time goes in v1:
time: 158 us; the launch traced here: 155 us
  Pallas kernels  150 us (95%)
  local copies, waits for them, and re-layouts  3.85 us (2%)
    pallas_call x1, Pallas kernels, local(): pl.pallas_call(body, out_shape=(jax.ShapeDtypeStruct(queries.shape, BF16)...  150 us
    unnamed x10, local copies, waits for them, and re-layouts  3.78 us

profile of v1, /device:TPU:24, one launch (start us, length us, event | category | flops | bytes accessed | tf_op | source)
XLA Modules:
  0.0 155.2 jit_solution(12453201546387544340)
XLA Ops:
  0.6 0.0 copy-start.3
  0.6 0.6 copy-done.3
  1.3 0.0 copy-start.1
  1.3 0.0 copy-start.2
  1.3 0.1 pad.3.clone
  1.4 0.6 copy-done.1
  2.0 0.0 copy-done.2
  2.0 0.7 maximum_maximum_fusion.small_ref
  2.6 150.0 %shard_map.131 = (bf16[2,64,1024]{2,1,0:T(8,128)(2,1)}, bf16[128,2048]{1,0:T(8,128)(2,1)}) custom-call(bf16[2,64,1024]{2,1,0:T(8,128)(2,1)} %q_hbm.1, bf16[2,64,1024]{2,1,0:T(8,128)(2,1)} %k_hbm.1, bf16[2,64,1024]{2,1,0:T(8,128)(2,1)} %v_hbm.1, f32[2,1,16384]{2,1,0:T(1,128)} %gate_ref.1, bf16[128,2048]{1,0:T(8,128)(2,1)} %x_ref.1, f32[1,2048]{1,0:T(1,128)} %bitcast.11, ...), custom_call_target="tpu_custom_call" | custom-call | tf_op jit(solution)/shard_map/pallas_call | solution.py:490
  152.7 0.0 copy-start
  152.7 1.7 %copy.16 = bf16[2,64,1024]{2,1,0:T(8,128)(2,1)} copy(bf16[2,64,1024]{2,1,0:T(8,128)(2,1)} %get-tuple-element.4) | data formatting | bytes 524288
  154.4 0.0 copy-done
  154.4 0.8 copy.17
  (2 shorter events, 0.0 us)
Async XLA Ops:
  0.6 0.7 copy-start.3
  1.3 0.7 copy-start.1
  1.3 0.7 copy-start.2
  152.7 1.7 %copy-start = (bf16[128,2048]{1,0:T(8,128)(2,1)S(1)}, bf16[128,2048]{1,0:T(8,128)(2,1)}, u32[]{:S(2)}) copy-start(bf16[128,2048]{1,0:T(8,128)(2,1)} %get-tuple-element.5) | copy-start | bytes 1572868
